TPU v7x, 32 devices: a whole 2x2x4 slice. The times are simulated.
32 devices in a mesh: sp: 16 (over z, y, x), tp: 2 (over core).
Axes of the slice: x: 2, y: 2, z: 4, core: 2. Of those that a mesh axis runs over, the one named last changes fastest.
Arguments:
- tokens: bfloat16 [4096, 2048], P('sp'), as said below
- in_gain: float32 [2048], replicated, may hold values from 0.1 to 1.9
- w_query: bfloat16 [2048, 1024], P(None, 'tp'), as said below
- w_key: bfloat16 [2048, 1024], P(None, 'tp'), may hold values from -0.125 to 0.125
- w_value: bfloat16 [2048, 1024], P(None, 'tp'), may hold values from -0.125 to 0.125
- lam: float32 [8], P('tp'), may hold values from 0.3 to 0.8
- sub_gain: float32 [128], replicated, may hold values from 0.1 to 1.9
- w_out: bfloat16 [1024, 2048], P('tp'), may hold values from -0.1875 to 0.1875
Outputs:
- mixed: bfloat16 [4096, 2048], P('sp')
Inputs may be any that keep to these rules, and one draw needn't show every extreme that they name: tokens: normal entries plus, for each block of 64 tokens, a factor times one direction common to all tokens. w_query: independent normal entries.
All inputs are finite; a program needn't handle non-finite values.
Results may differ from a plain program's by a relative error of at most 0.025.
The roundings to bfloat16 on the way count: a program that leaves them out, or rounds other values in their place, can miss the bound.
Values may be sent and summed in bfloat16 or wider, within the bound.
No kernel may reach another device: no remote copies, remote signals or barrier semaphores. Data moves between devices by JAX's collectives and lax.ppermute only.
A program may use at most 64 MiB of HBM per device.

v0:
```python
import jax
import jax.numpy as jnp
from jax import lax
from jax.sharding import PartitionSpec as P

KD = 64
VD = 128


def rotate(vectors, position):
    half = vectors.shape[-1] // 2
    freq = 500000.0 ** (-jnp.arange(0, 2 * half, 2, dtype=jnp.float32) / (2 * half))
    angle = position.astype(jnp.float32)[:, None] * freq[None, :]
    cosine = jnp.cos(angle)[:, None, :]
    sine = jnp.sin(angle)[:, None, :]
    first = vectors[..., :half]
    second = vectors[..., half:]
    return jnp.concatenate(
        [first * cosine - second * sine, second * cosine + first * sine], axis=-1
    )


def shards(tokens, in_gain, w_query, w_key, w_value, lam, sub_gain, w_out):
    span = tokens.shape[0]
    local_heads = lam.shape[0]
    xfloat = tokens.astype(jnp.float32)
    normed = (
        xfloat * lax.rsqrt(jnp.mean(xfloat * xfloat, axis=-1, keepdims=True) + 1e-06) * in_gain
    ).astype(jnp.bfloat16)
    weights_all = jnp.concatenate([w_query, w_key, w_value], axis=1)
    projected = jnp.dot(normed, weights_all, preferred_element_type=jnp.float32)
    qcols = local_heads * 2 * KD
    position = lax.axis_index("sp") * span + jnp.arange(span, dtype=jnp.int32)
    queries = rotate(projected[:, :qcols].reshape(span, 2 * local_heads, KD), position).astype(
        jnp.bfloat16
    )
    queries = queries.reshape(span, local_heads, 2, KD)
    keys = rotate(
        projected[:, qcols : 2 * qcols].reshape(span, 2 * local_heads, KD), position
    ).astype(jnp.bfloat16)
    keys = keys.reshape(span, qcols)
    values = projected[:, 2 * qcols :].astype(jnp.bfloat16)
    scale = KD ** (-0.5)

    def update(carry, key_piece, value_piece):
        top, mass, accum = carry
        count = key_piece.shape[0]
        key_four = key_piece.reshape(count, local_heads, 2, KD)
        value_three = value_piece.reshape(count, local_heads, VD)
        scores = (
            jnp.einsum("qhcd,khcd->hcqk", queries, key_four, preferred_element_type=jnp.float32)
            * scale
        )
        new_top = jnp.maximum(top, jnp.max(scores, axis=-1))
        factor = jnp.exp(top - new_top)
        expo = jnp.exp(scores - new_top[..., None])
        mass = mass * factor + jnp.sum(expo, axis=-1)
        weights = expo.astype(jnp.bfloat16)
        accum = accum * factor[..., None] + jnp.einsum(
            "hcqk,khe->hcqe", weights, value_three, preferred_element_type=jnp.float32
        )
        return (new_top, mass, accum)

    start_carry = (
        jnp.full((local_heads, 2, span), -1e30, jnp.float32),
        jnp.zeros((local_heads, 2, span), jnp.float32),
        jnp.zeros((local_heads, 2, span, VD), jnp.float32),
    )
    carry = start_carry
    key_piece = lax.all_gather(keys, "sp", axis=0, tiled=True)
    value_piece = lax.all_gather(values, "sp", axis=0, tiled=True)
    count = key_piece.shape[0]

    def step_block(inner, items):
        return (update(inner, items[0], items[1]), None)

    blocks = (
        key_piece.reshape(count // 512, 512, key_piece.shape[1]),
        value_piece.reshape(count // 512, 512, value_piece.shape[1]),
    )
    carry, unused = lax.scan(step_block, carry, blocks)
    top, mass, accum = carry
    read = accum / mass[..., None]
    diff = read[:, 0] - lam[:, None, None] * read[:, 1]
    normal = diff * lax.rsqrt(jnp.mean(diff * diff, axis=-1, keepdims=True) + 1e-05) * sub_gain
    attended = jnp.transpose(normal, (1, 0, 2)).reshape(span, local_heads * VD).astype(jnp.bfloat16)
    share = lax.psum_scatter(
        jnp.dot(attended, w_out, preferred_element_type=jnp.float32).astype(jnp.bfloat16),
        "tp",
        scatter_dimension=0,
        tiled=True,
    )
    result = lax.all_gather(share, "tp", axis=0, tiled=True)
    return result


def solution(mesh):
    in_specs = (
        P("sp", None),
        P(),
        P(None, "tp"),
        P(None, "tp"),
        P(None, "tp"),
        P("tp"),
        P(),
        P("tp", None),
    )
    out_specs = P("sp", None)
    return jax.shard_map(shards, mesh=mesh, in_specs=in_specs, out_specs=out_specs, check_vma=False)
```

profile of v0, /device:TPU:0, one launch (start us, length us, event | category | flops | bytes accessed | tf_op | source)
XLA Modules:
  0.0 281.3 jit_solution(3731221670889648921)
XLA Ops:
  6.6 1.7 fusion.19
  8.2 5.0 %fusion.13 = f32[256,1536]{1,0:T(8,128)S(1)} fusion(bf16[2048,512]{1,0:T(8,128)(2,1)} %param.14, bf16[2048,512]{1,0:T(8,128)(2,1)} %param.13, bf16[2048,512]{1,0:T(8,128)(2,1)} %param.12, bf16[256,2048]{1,0:T(8,128)(2,1)} %param.10, f32[2048]{0:T(1024)} %param.11, f32[256]{0:T(256)S(1)} %add_rsqrt_fusion.1), kind=kOutput, calls=%fused_computation.18 | convolution fusion | flops 1631584256 | bytes 8922112 | tf_op jit(solution)/shard_map/dot_general | solution.py:31
  17.2 1.8 slice.71
  19.2 87.7 %all-gather.4.cloned.1.call-done = bf16[4096,512]{0,1:T(8,128)(2,1)} async-done(((bf16[256,512]{0,1:T(8,128)(2,1)}), bf16[4096,512]{0,1:T(8,128)(2,1)}) %all-gather.4.cloned.1.call-update) | async-done | bytes 4194320 | tf_op jit(solution)/shard_map/all_gather | solution.py:70
  106.8 6.5 %copy.16 = bf16[4096,512]{1,0:T(8,128)(2,1)} copy(bf16[4096,512]{0,1:T(8,128)(2,1)} %all-gather.4.cloned.1.call-done) | data formatting | bytes 8388608 | tf_op jit(solution)/shard_map/all_gather | solution.py:70
  113.3 70.1 %all-gather.6.cloned.1.call-done = bf16[4096,512]{1,0:T(8,128)(2,1)} async-done(((bf16[256,512]{1,0:T(8,128)(2,1)}), bf16[4096,512]{1,0:T(8,128)(2,1)}) %all-gather.6.cloned.1.call-update) | async-done | bytes 4194320 | tf_op jit(solution)/shard_map/all_gather | solution.py:71
  183.4 66.4 %while.15 = (s32[]{:T(128)}, f32[4,2,256]{2,1,0:T(2,128)S(1)}, f32[4,2,256]{2,1,0:T(2,128)S(1)}, f32[4,2,256,128]{3,2,1,0:T(8,128)}, bf16[8,512,512]{2,1,0:T(8,1...) while((s32[]{:T(128)}, f32[4,2,256]{2,1,0:T(2,128)S(1)}, ...), condition=%wide.region_4.5_spmd.clone, body=%wide.region_1.4_spmd.clone.sunk | while | flops 411838464 | bytes 30802120 | solution.py:81
  183.4 2.1 constant_dynamic-slice_fusion.3
  185.5 1.3 copy.30
  189.4 1.4 fusion.49
  191.7 2.1 constant_dynamic-slice_fusion.3
  193.8 1.3 copy.30
  197.7 1.4 fusion.49
  200.0 2.1 constant_dynamic-slice_fusion.3
  202.1 1.3 copy.30
  206.0 1.4 fusion.49
  208.3 2.1 constant_dynamic-slice_fusion.3
  214.3 1.4 fusion.49
  216.6 2.1 constant_dynamic-slice_fusion.3
  218.7 1.3 copy.30
  222.6 1.4 fusion.49
  224.9 2.1 constant_dynamic-slice_fusion.3
  230.9 1.4 fusion.49
  233.3 2.1 constant_dynamic-slice_fusion.3
  239.2 1.4 fusion.49
  241.6 2.1 constant_dynamic-slice_fusion.3
  247.5 1.4 fusion.49
  249.9 1.6 copy.21
  251.9 1.7 convolution_convert_fusion
  253.7 7.1 %reduce-scatter.2.cloned.1.call-done = bf16[128,2048]{1,0:T(8,128)(2,1)} async-done(((bf16[256,2048]{1,0:T(8,128)(2,1)}), bf16[128,2048]{1,0:T(8,128)(2,1)}) %reduce-scatter.2.cloned.1.call-update) | async-done | bytes 524304 | tf_op jit(solution)/shard_map/reduce_scatter | solution.py:87
  260.8 11.7 %all-gather.8.cloned.1.call-done = bf16[256,2048]{1,0:T(8,128)(2,1)} async-done(((bf16[128,2048]{1,0:T(8,128)(2,1)}), bf16[256,2048]{1,0:T(8,128)(2,1)}) %all-gather.8.cloned.1.call-update) | async-done | bytes 1048592 | tf_op jit(solution)/shard_map/all_gather | solution.py:93
  272.5 2.3 copy.45
  (134 shorter events, 37.6 us)
Async XLA Ops:
  6.5 245.4 %copy-start = (bf16[512,2048]{1,0:T(8,128)(2,1)S(1)}, bf16[512,2048]{1,0:T(8,128)(2,1)}, u32[]{:S(2)}) copy-start(bf16[512,2048]{1,0:T(8,128)(2,1)} %param.17) | copy-start | bytes 6291460
  6.5 100.3 %all-gather.4.cloned.1.call-start = ((), (), s32[]{:S(2)}) async-start(), calls=%async_computation.1 | async-start | bytes 4456448 | tf_op jit(solution)/shard_map/all_gather | solution.py:70
  13.3 1.4 copy-start.4
  17.2 166.2 %all-gather.6.cloned.1.call-start = ((), (), s32[]{:S(2)}) async-start(), calls=%async_computation.2 | async-start | bytes 4456448 | tf_op jit(solution)/shard_map/all_gather | solution.py:71
  19.1 241.7 %reduce-scatter.2.cloned.1.call-start = ((), (), s32[]{:S(2)}) async-start(), calls=%async_computation.3 | async-start | bytes 1572864 | tf_op jit(solution)/shard_map/reduce_scatter | solution.py:87
  187.8 1.5 copy-start.1
  187.8 1.5 copy-start.2
  190.8 1.0 copy-start.3
  196.1 1.5 copy-start.1
  196.1 1.5 copy-start.2
  199.1 1.0 copy-start.3
  204.4 1.5 copy-start.1
  204.4 1.5 copy-start.2
  207.4 1.0 copy-start.3
  212.7 1.5 copy-start.1
  212.7 1.5 copy-start.2
  215.7 1.0 copy-start.3
  221.0 1.5 copy-start.1
  221.0 1.5 copy-start.2
  224.0 1.0 copy-start.3
  229.3 1.5 copy-start.1
  229.3 1.5 copy-start.2
  232.3 1.0 copy-start.3
  237.6 1.5 copy-start.1
  237.6 1.5 copy-start.2
  240.6 1.0 copy-start.3
  245.9 1.5 copy-start.1
  245.9 1.5 copy-start.2
  248.9 1.0 copy-start.3
  249.9 1.7 copy-start.5
  249.9 1.9 copy-start.6
  253.6 18.8 %all-gather.8.cloned.1.call-start = ((), (), s32[]{:S(2)}) async-start(), calls=%async_computation.4 | async-start | bytes 1572864 | tf_op jit(solution)/shard_map/all_gather | solution.py:93
Sparse Core Ops, SparseCore 0:
  17.3 89.4 all-gather.3
  109.6 73.7 all-gather.5
  253.8 6.9 reduce-scatter.1
  262.2 10.2 all-gather.7
where the time goes:
time: 282 us; the launch traced here: 281 us
  waiting for transfers between devices  177 us (63%)
  local copies, waits for them, and re-layouts  57.7 us (20%)
  matrix products  24.1 us (9%)
  between operations  13.3 us (5%)
  other arithmetic  9.1 us (3%)
    all_gather x1, waiting for transfers between devices, shards(): key_piece = lax.all_gather(keys, 'sp', axis=0, tiled=True)  87.7 us
    all_gather x1, waiting for transfers between devices, shards(): value_piece = lax.all_gather(values, 'sp', axis=0, tiled=True)  70.1 us
    dynamic_slice x24, local copies, waits for them, and re-layouts, shards(): carry, unused = lax.scan(step_block, carry, blocks)  35 us
    all_gather x1, waiting for transfers between devices, shards(): result = lax.all_gather(share, 'tp', axis=0, tiled=True)  11.7 us
    dot_general x8, matrix products, update(): jnp.einsum('hcqk,khe->hcqe', weights, value_three, preferred_element_type...  11.1 us
    while x56, local copies, waits for them, and re-layouts  7.71 us
    reduce_scatter x1, waiting for transfers between devices, shards(): lax.psum_scatter(jnp.dot(attended, w_out, preferred_element_type=jnp.floa...  7.07 us
    all_gather x1, local copies, waits for them, and re-layouts, shards(): key_piece = lax.all_gather(keys, 'sp', axis=0, tiled=True)  6.49 us
  transfers between devices with their start and end apart: 4, of which 4 were waited for; matrix products, arithmetic and copies ran while one was open for 3% of the time, Pallas kernels for 0%

commit v1 on v0

--- a/solution.py
+++ b/solution.py
@@ -68,7 +68,9 @@
     )
     carry = start_carry
     key_piece = lax.all_gather(keys, "sp", axis=0, tiled=True)
-    value_piece = lax.all_gather(values, "sp", axis=0, tiled=True)
+    value_piece = jnp.concatenate(
+        lax.all_to_all(jnp.stack([values] * lax.axis_size("sp")), "sp", 0, 0), axis=0
+    )
     count = key_piece.shape[0]
 
     def step_block(inner, items):

time: 282 us -> 279 us (0.989)
  waiting for transfers between devices: 177 us -> 163 us
  starting transfers between devices: 0.13 us -> 8.61 us
    all_gather x1 -> x0, waiting for transfers between devices: 70.1 us -> none  [shards(): value_piece = lax.all_gather(values, 'sp', axis=0, tiled=True)]
    all_gather x1, waiting for transfers between devices: 87.7 us -> 140 us  [shards(): key_piece = lax.all_gather(keys, 'sp', axis=0, tiled=True)]
    all_to_all x0 -> x1, starting transfers between devices: none -> 8.53 us  [shards(): lax.all_to_all(jnp.stack([values] * lax.axis_size('sp')), 'sp', 0, 0)]
    reduce_scatter x1, waiting for transfers between devices: 7.07 us -> 10.4 us  [shards(): lax.psum_scatter(jnp.dot(attended, w_out, preferred_element_type=jnp.floa...]
  transfers between devices with their start and end apart: 4 -> 4, of which waited for: 4 -> 3; matrix products, arithmetic and copies ran while one was open for 3% -> 4% of each run, Pallas kernels for 0% -> 0%
where the time goes in v1:
time: 279 us; the launch traced here: 278 us
  waiting for transfers between devices  163 us (58%)
  local copies, waits for them, and re-layouts  59.3 us (21%)
  matrix products  24.1 us (9%)
  between operations  13.3 us (5%)
  other arithmetic  9.75 us (3%)
  starting transfers between devices  8.61 us (3%)
    all_gather x1, waiting for transfers between devices, shards(): key_piece = lax.all_gather(keys, 'sp', axis=0, tiled=True)  140 us
    dynamic_slice x24, local copies, waits for them, and re-layouts, shards(): carry, unused = lax.scan(step_block, carry, blocks)  35 us
    all_gather x1, waiting for transfers between devices, shards(): result = lax.all_gather(share, 'tp', axis=0, tiled=True)  11.8 us
    dot_general x8, matrix products, update(): jnp.einsum('hcqk,khe->hcqe', weights, value_three, preferred_element_type...  11.1 us
    reduce_scatter x1, waiting for transfers between devices, shards(): lax.psum_scatter(jnp.dot(attended, w_out, preferred_element_type=jnp.floa...  10.4 us
    all_to_all x1, starting transfers between devices, shards(): lax.all_to_all(jnp.stack([values] * lax.axis_size('sp')), 'sp', 0, 0)  8.53 us
    while x56, local copies, waits for them, and re-layouts  7.71 us
    all_gather x1, local copies, waits for them, and re-layouts, shards(): key_piece = lax.all_gather(keys, 'sp', axis=0, tiled=True)  6.49 us
  transfers between devices with their start and end apart: 4, of which 3 were waited for; matrix products, arithmetic and copies ran while one was open for 4% of the time, Pallas kernels for 0%

profile of v1, /device:TPU:0, one launch (start us, length us, event | category | flops | bytes accessed | tf_op | source)
XLA Modules:
  0.0 278.0 jit_solution(15432155339395088410)
XLA Ops:
  6.6 1.7 fusion.19
  8.2 5.0 %fusion.13 = f32[256,1536]{1,0:T(8,128)S(1)} fusion(bf16[2048,512]{1,0:T(8,128)(2,1)} %param.14, bf16[2048,512]{1,0:T(8,128)(2,1)} %param.13, bf16[2048,512]{1,0:T(8,128)(2,1)} %param.12, bf16[256,2048]{1,0:T(8,128)(2,1)} %param.10, f32[2048]{0:T(1024)} %param.11, f32[256]{0:T(256)S(1)} %add_rsqrt_fusion.1), kind=kOutput, calls=%fused_computation.18 | convolution fusion | flops 1631584256 | bytes 8922112 | tf_op jit(solution)/shard_map/dot_general | solution.py:31
  18.9 2.3 stack.2
  21.2 8.5 %all-to-all-start = ((bf16[16,256,512]{2,1,0:T(8,128)(2,1)}), bf16[16,256,512]{2,1,0:T(8,128)(2,1)}, u32[]{:S(2)}, u32[]{:S(2)}) async-start(bf16[16,256,512]{2,1,0:T(8,128)(2,1)} %stack.2), calls=%async_computation | async-start | bytes 8388608 | tf_op jit(solution)/shard_map/all_to_all | solution.py:72
  29.9 140.2 %all-gather.3.cloned.1.call-done = bf16[4096,512]{0,1:T(8,128)(2,1)} async-done(((bf16[256,512]{0,1:T(8,128)(2,1)}), bf16[4096,512]{0,1:T(8,128)(2,1)}) %all-gather.3.cloned.1.call-update) | async-done | bytes 4194320 | tf_op jit(solution)/shard_map/all_gather | solution.py:70
  170.1 6.5 %copy.24 = bf16[4096,512]{1,0:T(8,128)(2,1)} copy(bf16[4096,512]{0,1:T(8,128)(2,1)} %all-gather.3.cloned.1.call-done) | data formatting | bytes 8388608 | tf_op jit(solution)/shard_map/all_gather | solution.py:70
  176.6 66.4 %while.15 = (s32[]{:T(128)}, f32[4,2,256]{2,1,0:T(2,128)S(1)}, f32[4,2,256]{2,1,0:T(2,128)S(1)}, f32[4,2,256,128]{3,2,1,0:T(8,128)}, bf16[8,512,512]{2,1,0:T(8,1...) while((s32[]{:T(128)}, f32[4,2,256]{2,1,0:T(2,128)S(1)}, ...), condition=%wide.region_4.5_spmd.clone, body=%wide.region_1.4_spmd.clone.sunk | while | flops 411838464 | bytes 30802120 | solution.py:83
  176.6 2.1 constant_dynamic-slice_fusion.3
  178.7 1.3 copy.38
  182.6 1.4 fusion.49
  184.9 2.1 constant_dynamic-slice_fusion.3
  187.0 1.3 copy.38
  190.9 1.4 fusion.49
  193.2 2.1 constant_dynamic-slice_fusion.3
  199.2 1.4 fusion.49
  201.5 2.1 constant_dynamic-slice_fusion.3
  203.6 1.3 copy.38
  207.5 1.4 fusion.49
  209.8 2.1 constant_dynamic-slice_fusion.3
  215.8 1.4 fusion.49
  218.1 2.1 constant_dynamic-slice_fusion.3
  224.1 1.4 fusion.49
  226.4 2.1 constant_dynamic-slice_fusion.3
  232.4 1.4 fusion.49
  234.8 2.1 constant_dynamic-slice_fusion.3
  236.8 1.3 copy.38
  240.7 1.4 fusion.49
  243.1 1.6 copy.29
  245.1 1.7 convolution_convert_fusion
  246.9 10.4 %reduce-scatter.2.cloned.1.call-done = bf16[128,2048]{1,0:T(8,128)(2,1)} async-done(((bf16[256,2048]{1,0:T(8,128)(2,1)}), bf16[128,2048]{1,0:T(8,128)(2,1)}) %reduce-scatter.2.cloned.1.call-update) | async-done | bytes 524304 | tf_op jit(solution)/shard_map/reduce_scatter | solution.py:89
  257.3 11.8 %all-gather.5.cloned.1.call-done = bf16[256,2048]{1,0:T(8,128)(2,1)} async-done(((bf16[128,2048]{1,0:T(8,128)(2,1)}), bf16[256,2048]{1,0:T(8,128)(2,1)}) %all-gather.5.cloned.1.call-update) | async-done | bytes 1048592 | tf_op jit(solution)/shard_map/all_gather | solution.py:95
  269.2 2.3 copy.53
  (136 shorter events, 39.3 us)
Async XLA Ops:
  6.5 238.6 %copy-start = (bf16[512,2048]{1,0:T(8,128)(2,1)S(1)}, bf16[512,2048]{1,0:T(8,128)(2,1)}, u32[]{:S(2)}) copy-start(bf16[512,2048]{1,0:T(8,128)(2,1)} %param.17) | copy-start | bytes 6291460
  6.5 163.6 %all-gather.3.cloned.1.call-start = ((), (), s32[]{:S(2)}) async-start(), calls=%async_computation.2 | async-start | bytes 4456448 | tf_op jit(solution)/shard_map/all_gather | solution.py:70
  13.3 1.4 copy-start.4
  21.2 8.6 %copy-start.5 = (bf16[256,8,32]{0,2,1:T(8,128)(2,1)S(1)}, bf16[256,8,32]{0,2,1:T(8,128)(2,1)}, u32[]{:S(2)}) copy-start(bf16[256,8,32]{0,2,1:T(8,128)(2,1)} %get-tuple-element.106) | copy-start | bytes 393220
  21.2 155.4 %all-to-all-start = ((bf16[16,256,512]{2,1,0:T(8,128)(2,1)}), bf16[16,256,512]{2,1,0:T(8,128)(2,1)}, u32[]{:S(2)}, u32[]{:S(2)}) async-start(bf16[16,256,512]{2,1,0:T(8,128)(2,1)} %stack.2), calls=%async_computation | async-start | bytes 8388608 | tf_op jit(solution)/shard_map/all_to_all | solution.py:72
  29.8 227.5 %reduce-scatter.2.cloned.1.call-start = ((), (), s32[]{:S(2)}) async-start(), calls=%async_computation.3 | async-start | bytes 1572864 | tf_op jit(solution)/shard_map/reduce_scatter | solution.py:89
  181.0 1.5 copy-start.1
  181.0 1.6 copy-start.2
  184.0 1.0 copy-start.3
  189.3 1.5 copy-start.1
  189.3 1.6 copy-start.2
  192.3 1.0 copy-start.3
  197.6 1.5 copy-start.1
  197.6 1.5 copy-start.2
  200.6 1.0 copy-start.3
  205.9 1.5 copy-start.1
  205.9 1.5 copy-start.2
  208.9 1.0 copy-start.3
  214.2 1.5 copy-start.1
  214.2 1.5 copy-start.2
  217.2 1.0 copy-start.3
  222.5 1.5 copy-start.1
  222.5 1.5 copy-start.2
  225.5 1.0 copy-start.3
  230.8 1.5 copy-start.1
  230.8 1.5 copy-start.2
  239.1 1.5 copy-start.1
  239.1 1.5 copy-start.2
  242.1 1.0 copy-start.3
  243.1 1.7 copy-start.6
  243.1 1.9 copy-start.7
  246.8 22.3 %all-gather.5.cloned.1.call-start = ((), (), s32[]{:S(2)}) async-start(), calls=%async_computation.4 | async-start | bytes 1572864 | tf_op jit(solution)/shard_map/all_gather | solution.py:95
  (1 other events, 1.0 us)
Sparse Core Ops, SparseCore 0:
  18.0 152.1 all-gather.2
  247.0 10.3 reduce-scatter.1
  258.9 10.2 all-gather.4
